TPU v7x, 32 devices: a whole 2x2x4 slice. The times are simulated.
32 devices in a mesh: sp: 8 (over z, x), tp: 4 (over y, core).
Axes of the slice: x: 2, y: 2, z: 4, core: 2. Of those that a mesh axis runs over, the one named last changes fastest.
Arguments:
- residual_matrix: bfloat16 [2048, 2048], P(('sp', 'tp')), may hold values from -6 to 6
- query_vectors: bfloat16 [2048, 2048], P('tp', 'sp'), may hold values from -6 to 6
- lookup_vectors: bfloat16 [2048, 2048], P('tp', 'sp'), may hold values from -6 to 6
- payload_vectors: bfloat16 [2048, 2048], P('tp', 'sp'), may hold values from -6 to 6
- fading_dependent_term: bfloat16 [2048, 2048], P('tp', 'sp'), may hold values from -4 to 4
- step_size_preactivation: bfloat16 [2048, 2048], P('tp', 'sp'), may hold values from -8 to 8
- attention_result_switch: bfloat16 [2048, 2048], P('tp', 'sp'), may hold values from -6 to 6
- fading_bias_vector: float32 [2048], P('tp'), may hold values from -16 to -2
- surplus_forgetting: float32 [32, 2048], P('tp', 'sp'), may hold values from -0.7 to 0
- per_group_scaler: float32 [2048], P('tp'), may hold values from 0.1 to 1.9
- attention_result_matrix: bfloat16 [2048, 2048], P('tp'), may hold values from -0.125 to 0.125
- dense_block_scaler: float32 [2048], replicated, may hold values from 0.1 to 1.9
- switching_matrix: bfloat16 [2048, 5632], P('sp', 'tp'), may hold values from -0.125 to 0.125
- expanding_matrix: bfloat16 [2048, 5632], P('sp', 'tp'), may hold values from -0.125 to 0.125
- contracting_matrix: bfloat16 [5632, 2048], P('tp', 'sp'), may hold values from -0.078125 to 0.078125
Outputs:
- blended: bfloat16 [2048, 2048], P(('sp', 'tp'))
All inputs are finite; a program needn't handle non-finite values.
Results may differ from a plain program's by a relative error of at most 0.015.
Values may be sent and summed in bfloat16 or wider, within the bound.
A program may use at most 128 MiB of HBM per device.

v0:
```python
import jax
import jax.numpy as jnp
from jax import lax
from jax.sharding import PartitionSpec as P

HEAD = 64
BLOCK = 64
norm_eps = 1e-06
group_eps = 0.00064
key_eps = 1e-06
highest = lax.Precision.HIGHEST


def carried_in(x, axis, join, neutral):
    place = lax.axis_index(axis)
    gathered = jax.tree.map(
        lambda a, kind: lax.all_gather(a.astype(kind), axis),
        x,
        jax.tree.map(lambda a: jnp.bfloat16 if a.dtype == jnp.float32 else a.dtype, x),
    )
    state = jax.tree.map(lambda a, e: jnp.zeros_like(a) + jnp.asarray(e, a.dtype), x, neutral)

    def one(turn, state):
        return join(
            state,
            jax.tree.map(
                lambda a, own: lax.dynamic_index_in_dim(a, turn, 0, False).astype(own.dtype),
                gathered,
                x,
            ),
        )

    return lax.fori_loop(0, place, one, state)


def by_blocks(source, attention_group_count, position_count):
    return (
        source.astype(jnp.float32)
        .reshape(attention_group_count, HEAD, position_count // BLOCK, BLOCK)
        .transpose(0, 2, 3, 1)
    )


def compose(earlier, latter):
    return (
        jnp.einsum("...ij,...jk->...ik", earlier[0], latter[0], precision=highest),
        jnp.einsum("...ij,...jk->...ik", earlier[1], latter[0], precision=highest) + latter[1],
    )


def unit_lower_solve(mutual, right_side):
    power = -mutual
    solved = right_side
    for level in range((BLOCK - 1).bit_length()):
        solved = solved + jnp.einsum("hbts,hbsn->hbtn", power, solved, precision=highest)
        if level + 1 < (BLOCK - 1).bit_length():
            power = jnp.einsum("hbts,hbsu->hbtu", power, power, precision=highest)
    return solved


def rms_rows(middle, dense_block_scaler):
    scale_rows = lax.rsqrt(jnp.mean(middle * middle, axis=-1, keepdims=True) + norm_eps)
    return (middle * scale_rows * dense_block_scaler).astype(jnp.bfloat16)


def local(
    residual_matrix,
    query_vectors,
    lookup_vectors,
    payload_vectors,
    fading_dependent_term,
    step_size_preactivation,
    attention_result_switch,
    fading_bias_vector,
    surplus_forgetting,
    per_group_scaler,
    attention_result_matrix,
    dense_block_scaler,
    switching_matrix,
    expanding_matrix,
    contracting_matrix,
):
    attention_group_count = surplus_forgetting.shape[0]
    position_count = surplus_forgetting.shape[1]
    block_count = position_count // BLOCK
    read_rows = by_blocks(query_vectors, attention_group_count, position_count)
    key_rows = by_blocks(lookup_vectors, attention_group_count, position_count)
    value_rows = by_blocks(payload_vectors, attention_group_count, position_count)
    fading_preactivation = by_blocks(
        fading_dependent_term, attention_group_count, position_count
    ) + fading_bias_vector.reshape(attention_group_count, 1, 1, HEAD)
    log_fading_factor = -jnp.exp(
        -jax.nn.softplus(-fading_preactivation) - 0.5
    ) + surplus_forgetting.reshape(attention_group_count, block_count, BLOCK, 1)
    learn_rate = jax.nn.sigmoid(
        by_blocks(step_size_preactivation, attention_group_count, position_count)
    )
    unit_keys = key_rows * lax.rsqrt(jnp.sum(key_rows * key_rows, axis=-1, keepdims=True) + key_eps)
    scaled = key_rows * learn_rate
    removal = unit_keys * learn_rate
    cum_after = jnp.cumsum(log_fading_factor, axis=2)
    before = cum_after - log_fading_factor
    cum_final = cum_after[:, :, -1:, :]
    probe_keys = unit_keys * jnp.exp(before)
    removal_in = removal * jnp.exp(-cum_after)
    scaled_in = scaled * jnp.exp(-cum_after)
    reads_out = read_rows * jnp.exp(cum_after)
    position = jnp.arange(BLOCK)
    strict = position[:, None] > position[None, :]
    up_to = position[:, None] >= position[None, :]
    mutual = jnp.where(
        strict, jnp.einsum("hbtn,hbsn->hbts", probe_keys, removal_in, precision=highest), 0.0
    )
    through = jnp.where(
        strict, jnp.einsum("hbtn,hbsn->hbts", probe_keys, scaled_in, precision=highest), 0.0
    )
    right_side = jnp.concatenate(
        [probe_keys, jnp.einsum("hbts,hbsn->hbtn", through, value_rows, precision=highest)], axis=-1
    )
    solved = unit_lower_solve(mutual, right_side)
    basis_part = solved[..., :HEAD]
    offset = solved[..., HEAD:]
    removal_end = removal * jnp.exp(cum_final - cum_after)
    scaled_end = scaled * jnp.exp(cum_final - cum_after)
    carry_map = jnp.eye(HEAD, dtype=jnp.float32) * jnp.exp(cum_final) - jnp.einsum(
        "hbtk,hbtj->hbkj", basis_part, removal_end, precision=highest
    )
    carry_add = jnp.einsum(
        "hbtv,hbtj->hbvj", value_rows, scaled_end, precision=highest
    ) - jnp.einsum("hbtv,hbtj->hbvj", offset, removal_end, precision=highest)
    block_maps = (jnp.moveaxis(carry_map, 1, 0), jnp.moveaxis(carry_add, 1, 0))
    identity = (
        jnp.broadcast_to(jnp.eye(HEAD, dtype=jnp.float32), (attention_group_count, HEAD, HEAD)),
        jnp.zeros((attention_group_count, HEAD, HEAD), jnp.float32),
    )

    def fold_step(total_map, member):
        return (compose(total_map, member), None)

    summary, _ = lax.scan(fold_step, identity, block_maps)
    _, entering = carried_in(summary, "sp", compose, identity)

    def walk_step(carried, member):
        moved_on = jnp.einsum("hvk,hkj->hvj", carried, member[0], precision=highest) + member[1]
        return (moved_on, carried)

    _, starts = lax.scan(walk_step, entering, block_maps)
    starts = jnp.moveaxis(starts, 0, 1)
    removed = -jnp.einsum("hbtk,hbvk->hbtv", basis_part, starts, precision=highest) - offset
    reach_removal = jnp.where(
        up_to, jnp.einsum("hbtn,hbsn->hbts", reads_out, removal_in, precision=highest), 0.0
    )
    reach_value = jnp.where(
        up_to, jnp.einsum("hbtn,hbsn->hbts", reads_out, scaled_in, precision=highest), 0.0
    )
    outputs = (
        jnp.einsum("hbtk,hbvk->hbtv", reads_out, starts, precision=highest)
        + jnp.einsum("hbts,hbsv->hbtv", reach_removal, removed, precision=highest)
        + jnp.einsum("hbts,hbsv->hbtv", reach_value, value_rows, precision=highest)
    )
    centred = outputs - jnp.mean(outputs, axis=-1, keepdims=True)
    normed_heads = centred * lax.rsqrt(
        jnp.mean(centred * centred, axis=-1, keepdims=True) + group_eps
    )
    normed_heads = normed_heads.transpose(0, 3, 1, 2).reshape(
        attention_group_count * HEAD, position_count
    )
    mixed_out = (
        normed_heads * per_group_scaler[:, None] * attention_result_switch.astype(jnp.float32)
    ).astype(jnp.bfloat16)
    moved_rows = lax.all_to_all(mixed_out, "tp", split_axis=1, concat_axis=0, tiled=True)
    whole_weight = lax.all_gather(attention_result_matrix, "tp", axis=0, tiled=True)
    middle = residual_matrix.astype(jnp.float32) + jnp.einsum(
        "ct,cd->td", moved_rows, whole_weight, preferred_element_type=jnp.float32
    )
    normed = rms_rows(middle, dense_block_scaler)
    all_rows = lax.all_gather(normed, "tp", axis=0, tiled=True)
    gate_sum = jnp.dot(
        all_rows,
        lax.all_gather(switching_matrix, "sp", axis=0, tiled=True),
        preferred_element_type=jnp.float32,
    )
    up_sum = jnp.dot(
        all_rows,
        lax.all_gather(expanding_matrix, "sp", axis=0, tiled=True),
        preferred_element_type=jnp.float32,
    )
    hidden = (jax.nn.silu(gate_sum) * up_sum).astype(jnp.bfloat16)
    down_full = lax.all_gather(contracting_matrix, "sp", axis=1, tiled=True)
    channel_out = lax.psum_scatter(
        jnp.dot(hidden, down_full, preferred_element_type=jnp.float32).astype(jnp.bfloat16),
        "tp",
        scatter_dimension=0,
        tiled=True,
    ).astype(jnp.float32)
    return (middle + channel_out).astype(jnp.bfloat16)


def solution(mesh):
    placed = (
        P(("sp", "tp"), None),
        P("tp", "sp"),
        P("tp", "sp"),
        P("tp", "sp"),
        P("tp", "sp"),
        P("tp", "sp"),
        P("tp", "sp"),
        P("tp"),
        P("tp", "sp"),
        P("tp"),
        P("tp", None),
        P(),
        P("sp", "tp"),
        P("sp", "tp"),
        P("tp", "sp"),
    )
    return jax.shard_map(
        local, mesh=mesh, in_specs=placed, out_specs=P(("sp", "tp"), None), check_vma=False
    )
```

profile of v0, /device:TPU:0, one launch (start us, length us, event | category | flops | bytes accessed | tf_op | source)
XLA Modules:
  0.0 466.2 jit_solution(5035272207007485328)
XLA Ops:
  19.5 3.8 fusion.46
  23.4 3.4 convolution_select_fusion.3
  26.8 2.8 fusion.23
  30.7 2.7 convolution_bitcast_fusion.6
  33.4 2.3 fusion.55
  50.6 2.1 fusion.21
  53.9 4.5 fusion.22
  58.4 2.5 copy.103
  61.0 17.9 %while.39 = (s32[]{:T(128)}, f32[8,64,64]{1,2,0:T(8,128)S(1)}, f32[8,64,64]{1,2,0:T(8,128)}, f32[4,8,64,64]{2,3,1,0:T(8,128)}, f32[4,8,64,64]{2,3,1,0:T(8,128)}, /*index=5*/s32[]{:T(128)}, s32[]{:T(128)}) while((s32[]{:T(128)}, f32[8,64,64]{1,2,0:T(8,128)S(1)}, f32[8,64,64]{1,2,0:T(8,128)}, f32[4,8,64,64]{2,3,1,0:T(8,128)}, ...), condition=%wide.region_3.4_spmd.clone, body=%wide.region_2.3_spmd.clone.sunk | while | flops 50397184 | bytes 1836631 | solution.py:140
  80.1 40.5 %all-gather = bf16[64,64,64]{2,1,0:T(8,128)(2,1)} all-gather(bf16[8,64,64]{2,1,0:T(8,128)(2,1)S(1)} %copy.105), channel_id=2, replica_groups=mesh['sp'=8,'tp'=4] {'sp'}, dimensions={0}, use_global_device_ids=true | all-gather | bytes 589824 | tf_op jit(solution)/shard_map/all_gather | solution.py:17
  120.7 39.5 %all-gather.1 = bf16[64,64,64]{2,1,0:T(8,128)(2,1)} all-gather(bf16[8,64,64]{2,1,0:T(8,128)(2,1)S(1)} %copy.106), channel_id=3, replica_groups=mesh['sp'=8,'tp'=4] {'sp'}, dimensions={0}, use_global_device_ids=true | all-gather | bytes 589824 | tf_op jit(solution)/shard_map/all_gather | solution.py:17
  160.1 8.8 %while.38 = (s32[]{:T(128)}, f32[8,64,64]{1,2,0:T(8,128)S(1)}, f32[4,8,64,64]{2,3,1,0:T(8,128)}, f32[4,8,64,64]{2,3,1,0:T(8,128)}, f32[4,8,64,64]{2,3,1,0:T(8,128)}, /*index=5*/s32[]{:T(128)}) while((s32[]{:T(128)}, f32[8,64,64]{1,2,0:T(8,128)S(1)}, f32[4,8,64,64]{2,3,1,0:T(8,128)}, f32[4,8,64,64]{2,3,1,0:T(8,128)}, ...), condition=%wide.region_7.8_spmd, body=%wide.region_6.7_spmd.sunk | while | flops 25198592 | bytes 1443397 | solution.py:147
  169.0 3.3 fusion.20
  172.2 3.9 fusion.44
  176.2 2.3 convolution_select_fusion.1
  180.5 3.2 convolution_select_fusion
  186.2 8.6 %all_to_all.19 = bf16[512,4,64]{0,2,1:T(8,128)(2,1)S(1)} all-to-all(bf16[512,4,64]{0,2,1:T(8,128)(2,1)S(1)} %bitcast.213), channel_id=1, replica_groups=mesh['sp'=8,'tp'=4] {'tp'}, dimensions={1} | all-to-all | bytes 524288 | tf_op jit(solution)/shard_map/all_to_all | solution.py:171
  194.9 5.1 %multiply_reduce_fusion.1 = (f32[64]{0:T(128)S(1)}, f32[64,2048]{1,0:T(8,128)S(1)}) fusion(bf16[2048,64]{0,1:T(8,128)(2,1)S(1)} %bitcast.211, bf16[2048,2048]{1,0:T(8,128)(2,1)} %all-gather.8.cloned.1.call-done, bf16[64,2048]{1,0:T(8,128)(2,1)S(1)} %copy-done.10), kind=kOutput, calls=%fused_computation.97 | convolution fusion | flops 537395136 | bytes 9437440 | tf_op jit(solution)/shard_map/ct,cd->td/dot_general | solution.py:173
  202.0 35.8 %all-gather.10.cloned.1.call-done = bf16[256,2048]{1,0:T(8,128)(2,1)} async-done(((bf16[64,2048]{1,0:T(8,128)(2,1)}), bf16[256,2048]{1,0:T(8,128)(2,1)}) %all-gather.10.cloned.1.call-update) | async-done | bytes 1048592 | tf_op jit(solution)/shard_map/all_gather | solution.py:177
  237.8 4.8 %fusion.72 = f32[256,1408]{1,0:T(8,128)S(1)} fusion(bf16[256,2048]{1,0:T(8,128)(2,1)} %all-gather.10.cloned.1.call-done, bf16[2048,1408]{1,0:T(8,128)(2,1)} %all-gather.12.cloned.1.call-done), kind=kOutput, calls=%fused_computation.122 | convolution fusion | flops 1476395008 | bytes 8257536 | tf_op jit(solution)/shard_map/dot_general | solution.py:178
  242.7 89.5 %all-gather.14.cloned.1.call-done = bf16[2048,1408]{1,0:T(8,128)(2,1)} async-done(((bf16[256,1408]{1,0:T(8,128)(2,1)}), bf16[2048,1408]{1,0:T(8,128)(2,1)}) %all-gather.14.cloned.1.call-update) | async-done | bytes 5767184 | tf_op jit(solution)/shard_map/all_gather | solution.py:185
  332.2 93.2 %all-gather.16.cloned.1.call-done = bf16[1408,2048]{1,0:T(8,128)(2,1)} async-done(((bf16[1408,256]{1,0:T(8,128)(2,1)}), bf16[1408,2048]{1,0:T(8,128)(2,1)}) %all-gather.16.cloned.1.call-update) | async-done | bytes 5767184 | tf_op jit(solution)/shard_map/all_gather | solution.py:189
  425.4 8.8 %convolution_convert_fusion = bf16[256,2048]{1,0:T(8,128)(2,1)} fusion(bf16[1408,2048]{1,0:T(8,128)(2,1)} %all-gather.16.cloned.1.call-done, bf16[256,2048]{1,0:T(8,128)(2,1)S(1)} %copy-done.19, bf16[2048,1408]{1,0:T(8,128)(2,1)} %all-gather.14.cloned.1.call-done, f32[256,1408]{1,0:T(8,128)S(1)} %fusion.72), kind=kOutput, calls=%fused_computation.28 | convolution fusion | flops 2955476992 | bytes 15073280 | tf_op jit(solution)/shard_map/dot_general | solution.py:191
  434.3 23.1 %reduce-scatter.2.cloned.1.call-done = bf16[64,2048]{1,0:T(8,128)(2,1)} async-done(((bf16[256,2048]{1,0:T(8,128)(2,1)}), bf16[64,2048]{1,0:T(8,128)(2,1)}) %reduce-scatter.2.cloned.1.call-update) | async-done | bytes 262160 | tf_op jit(solution)/shard_map/reduce_scatter | solution.py:190
  (138 shorter events, 65.8 us)
Async XLA Ops:
  6.5 3.3 copy-start.16
  6.5 3.4 copy-start.18
  6.5 3.5 copy-start.11
  6.5 188.3 %all-gather.8.cloned.1.call-start = ((), (), s32[]{:S(2)}) async-start(), calls=%async_computation.2 | async-start | bytes 10485760 | tf_op jit(solution)/shard_map/all_gather | solution.py:172
  7.3 194.8 %all-gather.12.cloned.1.call-start = ((), (), s32[]{:S(2)}) async-start(), calls=%async_computation.4 | async-start | bytes 6488064 | tf_op jit(solution)/shard_map/all_gather | solution.py:180
  8.0 229.8 %all-gather.10.cloned.1.call-start = ((), (), s32[]{:S(2)}) async-start(), calls=%async_computation.3 | async-start | bytes 1310720 | tf_op jit(solution)/shard_map/all_gather | solution.py:177
  9.5 4.5 copy-start.12
  23.3 3.5 copy-start.2
  23.3 3.5 copy-start.5
  23.4 6.2 %copy-start.13 = (bf16[512,256]{1,0:T(8,128)(2,1)S(1)}, bf16[512,256]{1,0:T(8,128)(2,1)}, u32[]{:S(2)}) copy-start(bf16[512,256]{1,0:T(8,128)(2,1)} %param.24) | copy-start | bytes 786436
  30.7 5.1 %copy-start.4 = (f32[8,4,64,64]{3,2,1,0:T(8,128)S(1)}, f32[8,4,64,64]{3,2,1,0:T(8,128)}, u32[]{:S(2)}) copy-start(f32[8,4,64,64]{3,2,1,0:T(8,128)} %fusion.23) | copy-start | bytes 1572868
  30.7 6.3 %copy-start.3 = (f32[8,4,64,64]{3,2,1,0:T(8,128)S(1)}, f32[8,4,64,64]{3,2,1,0:T(8,128)}, u32[]{:S(2)}) copy-start(f32[8,4,64,64]{3,2,1,0:T(8,128)} %copy-done.2) | copy-start | bytes 1572868
  44.8 5.8 %copy-start.7 = (f32[8,4,64,64]{3,2,1,0:T(8,128)S(1)}, f32[8,4,64,64]{3,2,1,0:T(8,128)}, u32[]{:S(2)}) copy-start(f32[8,4,64,64]{3,2,1,0:T(8,128)} %get-tuple-element.192) | copy-start | bytes 1572868
  169.0 7.2 %copy-start = (f32[8,4,64,64]{3,0,1,2:T(8,128)S(1)}, f32[8,4,64,64]{3,0,1,2:T(8,128)}, u32[]{:S(2)}) copy-start(f32[8,4,64,64]{3,0,1,2:T(8,128)} %get-tuple-element.196) | copy-start | bytes 1572868
  169.0 7.2 %copy-start.6 = (f32[8,4,64,64]{3,2,1,0:T(8,128)S(1)}, f32[8,4,64,64]{3,2,1,0:T(8,128)}, u32[]{:S(2)}) copy-start(f32[8,4,64,64]{3,2,1,0:T(8,128)} %copy-done.5) | copy-start | bytes 1572868
  176.2 7.5 %copy-start.9 = (bf16[8,64,4,64]{3,2,1,0:T(4,128)(2,1)S(1)}, bf16[8,64,4,64]{3,2,1,0:T(4,128)(2,1)}, u32[]{:S(2)}) copy-start(bf16[8,64,4,64]{3,2,1,0:T(4,128)(2,1)} %reshape.74) | copy-start | bytes 786436
  183.7 2.3 copy-start.14
  183.7 2.5 copy-start.17
  183.7 11.2 %copy-start.10 = (bf16[64,2048]{1,0:T(8,128)(2,1)S(1)}, bf16[64,2048]{1,0:T(8,128)(2,1)}, u32[]{:S(2)}) copy-start(bf16[64,2048]{1,0:T(8,128)(2,1)} %param.21) | copy-start | bytes 786436
  194.8 5.1 %copy-start.15 = (f32[2048]{0:T(1024)S(1)}, f32[2048]{0:T(1024)}, u32[]{:S(2)}) copy-start(f32[2048]{0:T(1024)} %param.32) | copy-start | bytes 24580
  200.8 131.4 %all-gather.14.cloned.1.call-start = ((), (), s32[]{:S(2)}) async-start(), calls=%async_computation.5 | async-start | bytes 6488064 | tf_op jit(solution)/shard_map/all_gather | solution.py:185
  201.4 224.0 %all-gather.16.cloned.1.call-start = ((), (), s32[]{:S(2)}) async-start(), calls=%async_computation.6 | async-start | bytes 6488064 | tf_op jit(solution)/shard_map/all_gather | solution.py:189
  202.0 255.4 %reduce-scatter.2.cloned.1.call-start = ((), (), s32[]{:S(2)}) async-start(), calls=%async_computation.7 | async-start | bytes 1310720 | tf_op jit(solution)/shard_map/reduce_scatter | solution.py:190
  237.8 187.6 %copy-start.19 = (bf16[256,2048]{1,0:T(8,128)(2,1)S(1)}, bf16[256,2048]{1,0:T(8,128)(2,1)}, u32[]{:S(2)}) copy-start(bf16[256,2048]{1,0:T(8,128)(2,1)} %all-gather.10.cloned.1.call-done) | copy-start | bytes 3145732
  (2 other events, 2.6 us)
Sparse Core Ops, SparseCore 0:
  8.9 60.9 all-gather.7
  72.1 118.7 all-gather.11
  200.9 36.8 all-gather.9
  239.9 92.2 all-gather.13
  334.1 91.2 all-gather.15
  434.4 22.9 reduce-scatter.1
where the time goes:
time: 472 us; the launch traced here: 466 us
  waiting for transfers between devices  244 us (52%)
  blocking collectives  88.6 us (19%)
  matrix products  85.6 us (18%)
  local copies, waits for them, and re-layouts  22.1 us (5%)
  between operations  14.3 us (3%)
  other arithmetic  11.1 us (2%)
    all_gather x1, waiting for transfers between devices, local(): down_full = lax.all_gather(contracting_matrix, 'sp', axis=1, tiled=True)  93.2 us
    all_gather x1, waiting for transfers between devices, local(): lax.all_gather(expanding_matrix, 'sp', axis=0, tiled=True)  89.5 us
    all_gather x2, blocking collectives, carried_in(): lax.all_gather(a.astype(kind), axis)  80 us
    all_gather x1, waiting for transfers between devices, local(): all_rows = lax.all_gather(normed, 'tp', axis=0, tiled=True)  35.8 us
    reduce_scatter x1, waiting for transfers between devices, local(): lax.psum_scatter(jnp.dot(hidden, down_full, preferred_element_type=jnp.fl...  23.1 us
  transfers between devices with their start and end apart: 6, of which 4 were waited for; matrix products, arithmetic and copies ran while one was open for 23% of the time, Pallas kernels for 0%

commit v1 on v0

--- a/solution.py
+++ b/solution.py
@@ -1,3 +1,4 @@
+import functools
 import jax
 import jax.numpy as jnp
 from jax import lax
@@ -9,6 +10,14 @@
 group_eps = 0.00064
 key_eps = 1e-06
 highest = lax.Precision.HIGHEST
+
+
+def assign_series(x_in, dev_axis, d_out):
+    piece_out = jnp.concatenate(jax.lax.all_gather(x_in, dev_axis), d_out)
+    return piece_out
+
+
+limits_save = functools.partial(assign_series, dev_axis="sp", d_out=1)
 
 
 def carried_in(x, axis, join, neutral):
@@ -186,7 +195,7 @@
         preferred_element_type=jnp.float32,
     )
     hidden = (jax.nn.silu(gate_sum) * up_sum).astype(jnp.bfloat16)
-    down_full = lax.all_gather(contracting_matrix, "sp", axis=1, tiled=True)
+    down_full = limits_save(contracting_matrix)
     channel_out = lax.psum_scatter(
         jnp.dot(hidden, down_full, preferred_element_type=jnp.float32).astype(jnp.bfloat16),
         "tp",

time: 472 us -> 443 us (0.939)
  waiting for transfers between devices: 244 us -> 206 us
  local copies, waits for them, and re-layouts: 22.1 us -> 30.5 us
    all_gather x1, waiting for transfers between devices: 93.2 us -> 0.02 us  [assign_series(): piece_out = jnp.concatenate(jax.lax.all_gather(x_in, dev_axis), d_out)]
    all_gather x1, waiting for transfers between devices: 0.02 us -> 74.3 us  [local(): lax.all_gather(switching_matrix, 'sp', axis=0, tiled=True)]
    all_gather x1, waiting for transfers between devices: 35.8 us -> 16.3 us  [local(): all_rows = lax.all_gather(normed, 'tp', axis=0, tiled=True)]
    reshape x0 -> x1, local copies, waits for them, and re-layouts: none -> 8.32 us  [assign_series(): piece_out = jnp.concatenate(jax.lax.all_gather(x_in, dev_axis), d_out)]
  transfers between devices with their start and end apart: 6 -> 6, of which waited for: 4 -> 4; matrix products, arithmetic and copies ran while one was open for 23% -> 27% of each run, Pallas kernels for 0% -> 0%
where the time goes in v1:
time: 443 us; the launch traced here: 436 us
  waiting for transfers between devices  206 us (47%)
  blocking collectives  88.1 us (20%)
  matrix products  85.7 us (19%)
  local copies, waits for them, and re-layouts  30.5 us (7%)
  between operations  14.3 us (3%)
  other arithmetic  11 us (2%)
    all_gather x1, waiting for transfers between devices, local(): lax.all_gather(expanding_matrix, 'sp', axis=0, tiled=True)  89.5 us
    all_gather x2, blocking collectives, carried_in(): lax.all_gather(a.astype(kind), axis)  79.6 us
    all_gather x1, waiting for transfers between devices, local(): lax.all_gather(switching_matrix, 'sp', axis=0, tiled=True)  74.3 us
    reduce_scatter x1, waiting for transfers between devices, local(): lax.psum_scatter(jnp.dot(hidden, down_full, preferred_element_type=jnp.fl...  23.2 us
    all_gather x1, waiting for transfers between devices, local(): all_rows = lax.all_gather(normed, 'tp', axis=0, tiled=True)  16.3 us
  transfers between devices with their start and end apart: 6, of which 4 were waited for; matrix products, arithmetic and copies ran while one was open for 27% of the time, Pallas kernels for 0%

profile of v1, /device:TPU:0, one launch (start us, length us, event | category | flops | bytes accessed | tf_op | source)
XLA Modules:
  0.0 436.1 jit_solution(14488553108037863280)
XLA Ops:
  20.2 3.8 fusion.46
  24.1 3.5 convolution_select_fusion.3
  27.5 2.9 fusion.23
  31.5 2.7 convolution_bitcast_fusion.6
  34.2 2.3 fusion.55
  54.8 4.5 %fusion.22 = f32[4,8,64,64]{3,2,0,1:T(8,128)} fusion(f32[8,4,64,64]{3,2,1,0:T(8,128)} %get-tuple-element.202, f32[8,4,64,128]{3,2,1,0:T(8,128)} %copy-done.1, f32[4,8,64]{2,0,1:T(4,128)S(1)} %copy.127, f32[64,64]{1,0:T(8,128)S(1)} %fusion.61), kind=kOutput, calls=%fused_computation.43 | convolution fusion | flops 100925440 | bytes 2121728 | tf_op jit(solution)/shard_map/hbtk,hbtj->hbkj/dot_general | solution.py:134
  59.4 2.6 copy.143
  62.0 17.9 %while.39 = (s32[]{:T(128)}, f32[8,64,64]{1,2,0:T(8,128)S(1)}, f32[8,64,64]{1,2,0:T(8,128)}, f32[4,8,64,64]{2,3,1,0:T(8,128)}, f32[4,8,64,64]{2,3,1,0:T(8,128)}, /*index=5*/s32[]{:T(128)}, s32[]{:T(128)}) while((s32[]{:T(128)}, f32[8,64,64]{1,2,0:T(8,128)S(1)}, f32[8,64,64]{1,2,0:T(8,128)}, f32[4,8,64,64]{2,3,1,0:T(8,128)}, ...), condition=%wide.region_3.4_spmd.clone, body=%wide.region_2.3_spmd.clone.sunk | while | flops 50397184 | bytes 1836631 | solution.py:149
  81.1 40.1 %all-gather = bf16[64,64,64]{2,1,0:T(8,128)(2,1)} all-gather(bf16[8,64,64]{2,1,0:T(8,128)(2,1)S(1)} %copy.145), channel_id=2, replica_groups=mesh['sp'=8,'tp'=4] {'sp'}, dimensions={0}, use_global_device_ids=true | all-gather | bytes 589824 | tf_op jit(solution)/shard_map/all_gather | solution.py:26
  121.3 39.5 %all-gather.1 = bf16[64,64,64]{2,1,0:T(8,128)(2,1)} all-gather(bf16[8,64,64]{2,1,0:T(8,128)(2,1)S(1)} %copy.146), channel_id=3, replica_groups=mesh['sp'=8,'tp'=4] {'sp'}, dimensions={0}, use_global_device_ids=true | all-gather | bytes 589824 | tf_op jit(solution)/shard_map/all_gather | solution.py:26
  160.8 8.8 %while.38 = (s32[]{:T(128)}, f32[8,64,64]{1,2,0:T(8,128)S(1)}, f32[4,8,64,64]{2,3,1,0:T(8,128)}, f32[4,8,64,64]{2,3,1,0:T(8,128)}, f32[4,8,64,64]{2,3,1,0:T(8,128)}, /*index=5*/s32[]{:T(128)}) while((s32[]{:T(128)}, f32[8,64,64]{1,2,0:T(8,128)S(1)}, f32[4,8,64,64]{2,3,1,0:T(8,128)}, f32[4,8,64,64]{2,3,1,0:T(8,128)}, ...), condition=%wide.region_7.8_spmd, body=%wide.region_6.7_spmd.sunk | while | flops 25198592 | bytes 1443397 | solution.py:156
  169.6 3.3 fusion.20
  172.9 3.9 fusion.44
  176.8 2.3 convolution_select_fusion.1
  181.1 3.2 convolution_select_fusion
  186.9 8.4 %all_to_all.19 = bf16[512,4,64]{0,2,1:T(8,128)(2,1)S(1)} all-to-all(bf16[512,4,64]{0,2,1:T(8,128)(2,1)S(1)} %bitcast.219), channel_id=1, replica_groups=mesh['sp'=8,'tp'=4] {'tp'}, dimensions={1} | all-to-all | bytes 524288 | tf_op jit(solution)/shard_map/all_to_all | solution.py:180
  195.4 5.1 %multiply_reduce_fusion.1 = (f32[64]{0:T(128)S(1)}, f32[64,2048]{1,0:T(8,128)S(1)}) fusion(bf16[2048,64]{0,1:T(8,128)(2,1)S(1)} %bitcast.217, bf16[2048,2048]{1,0:T(8,128)(2,1)} %all-gather.9.cloned.1.call-done, bf16[64,2048]{1,0:T(8,128)(2,1)S(1)} %copy-done.10), kind=kOutput, calls=%fused_computation.97 | convolution fusion | flops 537395136 | bytes 9437440 | tf_op jit(solution)/shard_map/ct,cd->td/dot_general | solution.py:182
  202.0 8.3 %copy.160 = bf16[1408,8,256]{0,2,1:T(8,128)(2,1)} copy(bf16[1408,8,256]{2,0,1:T(8,128)(2,1)} %bitcast.213) | data formatting | bytes 11534336 | tf_op jit(solution)/shard_map/reshape | solution.py:16
  210.3 74.3 %all-gather.13.cloned.1.call-done = bf16[2048,1408]{1,0:T(8,128)(2,1)} async-done(((bf16[256,1408]{1,0:T(8,128)(2,1)}), bf16[2048,1408]{1,0:T(8,128)(2,1)}) %all-gather.13.cloned.1.call-update) | async-done | bytes 5767184 | tf_op jit(solution)/shard_map/all_gather | solution.py:189
  284.6 16.3 %all-gather.11.cloned.1.call-done = bf16[256,2048]{1,0:T(8,128)(2,1)} async-done(((bf16[64,2048]{1,0:T(8,128)(2,1)}), bf16[256,2048]{1,0:T(8,128)(2,1)}) %all-gather.11.cloned.1.call-update) | async-done | bytes 1048592 | tf_op jit(solution)/shard_map/all_gather | solution.py:186
  301.0 4.8 %fusion.72 = f32[256,1408]{1,0:T(8,128)S(1)} fusion(bf16[256,2048]{1,0:T(8,128)(2,1)} %all-gather.11.cloned.1.call-done, bf16[2048,1408]{1,0:T(8,128)(2,1)} %all-gather.13.cloned.1.call-done), kind=kOutput, calls=%fused_computation.122 | convolution fusion | flops 1476395008 | bytes 8257536 | tf_op jit(solution)/shard_map/dot_general | solution.py:187
  305.8 89.5 %all-gather.15.cloned.1.call-done = bf16[2048,1408]{1,0:T(8,128)(2,1)} async-done(((bf16[256,1408]{1,0:T(8,128)(2,1)}), bf16[2048,1408]{1,0:T(8,128)(2,1)}) %all-gather.15.cloned.1.call-update) | async-done | bytes 5767184 | tf_op jit(solution)/shard_map/all_gather | solution.py:194
  395.3 8.8 %convolution_convert_fusion = bf16[256,2048]{1,0:T(8,128)(2,1)} fusion(bf16[1408,2048]{0,1:T(8,128)(2,1)} %bitcast.214, bf16[256,2048]{1,0:T(8,128)(2,1)S(1)} %copy-done.19, bf16[2048,1408]{1,0:T(8,128)(2,1)} %all-gather.15.cloned.1.call-done, f32[256,1408]{1,0:T(8,128)S(1)} %fusion.72), kind=kOutput, calls=%fused_computation.28 | convolution fusion | flops 2955476992 | bytes 15073280 | tf_op jit(solution)/shard_map/dot_general | solution.py:200
  404.2 23.2 %reduce-scatter.2.cloned.1.call-done = bf16[64,2048]{1,0:T(8,128)(2,1)} async-done(((bf16[256,2048]{1,0:T(8,128)(2,1)}), bf16[64,2048]{1,0:T(8,128)(2,1)}) %reduce-scatter.2.cloned.1.call-update) | async-done | bytes 262160 | tf_op jit(solution)/shard_map/reduce_scatter | solution.py:199
  (139 shorter events, 68.1 us)
Async XLA Ops:
  6.5 4.1 copy-start.16
  6.5 4.2 copy-start.18
  6.5 4.2 copy-start.11
  6.5 188.8 %all-gather.9.cloned.1.call-start = ((), (), s32[]{:S(2)}) async-start(), calls=%async_computation.2 | async-start | bytes 10485760 | tf_op jit(solution)/shard_map/all_gather | solution.py:181
  7.3 194.7 %all-gather.17.cloned.1.call-start = ((), (), s32[]{:S(2)}) async-start(), calls=%async_computation.7 | async-start | bytes 6488064 | tf_op jit(solution)/shard_map/all_gather | solution.py:16
  8.0 276.6 %all-gather.13.cloned.1.call-start = ((), (), s32[]{:S(2)}) async-start(), calls=%async_computation.4 | async-start | bytes 6488064 | tf_op jit(solution)/shard_map/all_gather | solution.py:189
  8.7 292.2 %all-gather.11.cloned.1.call-start = ((), (), s32[]{:S(2)}) async-start(), calls=%async_computation.3 | async-start | bytes 1310720 | tf_op jit(solution)/shard_map/all_gather | solution.py:186
  10.3 4.5 %copy-start.12 = (bf16[512,256]{1,0:T(8,128)(2,1)S(1)}, bf16[512,256]{1,0:T(8,128)(2,1)}, u32[]{:S(2)}) copy-start(bf16[512,256]{1,0:T(8,128)(2,1)} %param.23) | copy-start | bytes 786436
  24.0 3.5 copy-start.2
  24.0 3.5 copy-start.5
  24.0 6.4 %copy-start.13 = (bf16[512,256]{1,0:T(8,128)(2,1)S(1)}, bf16[512,256]{1,0:T(8,128)(2,1)}, u32[]{:S(2)}) copy-start(bf16[512,256]{1,0:T(8,128)(2,1)} %param.24) | copy-start | bytes 786436
  31.5 5.1 %copy-start.4 = (f32[8,4,64,64]{3,2,1,0:T(8,128)S(1)}, f32[8,4,64,64]{3,2,1,0:T(8,128)}, u32[]{:S(2)}) copy-start(f32[8,4,64,64]{3,2,1,0:T(8,128)} %fusion.23) | copy-start | bytes 1572868
  31.5 6.3 %copy-start.3 = (f32[8,4,64,64]{3,2,1,0:T(8,128)S(1)}, f32[8,4,64,64]{3,2,1,0:T(8,128)}, u32[]{:S(2)}) copy-start(f32[8,4,64,64]{3,2,1,0:T(8,128)} %copy-done.2) | copy-start | bytes 1572868
  45.6 5.8 %copy-start.7 = (f32[8,4,64,64]{3,2,1,0:T(8,128)S(1)}, f32[8,4,64,64]{3,2,1,0:T(8,128)}, u32[]{:S(2)}) copy-start(f32[8,4,64,64]{3,2,1,0:T(8,128)} %get-tuple-element.202) | copy-start | bytes 1572868
  169.6 7.2 %copy-start = (f32[8,4,64,64]{3,0,1,2:T(8,128)S(1)}, f32[8,4,64,64]{3,0,1,2:T(8,128)}, u32[]{:S(2)}) copy-start(f32[8,4,64,64]{3,0,1,2:T(8,128)} %get-tuple-element.206) | copy-start | bytes 1572868
  169.6 7.2 %copy-start.6 = (f32[8,4,64,64]{3,2,1,0:T(8,128)S(1)}, f32[8,4,64,64]{3,2,1,0:T(8,128)}, u32[]{:S(2)}) copy-start(f32[8,4,64,64]{3,2,1,0:T(8,128)} %copy-done.5) | copy-start | bytes 1572868
  176.8 7.5 %copy-start.9 = (bf16[8,64,4,64]{3,2,1,0:T(4,128)(2,1)S(1)}, bf16[8,64,4,64]{3,2,1,0:T(4,128)(2,1)}, u32[]{:S(2)}) copy-start(bf16[8,64,4,64]{3,2,1,0:T(4,128)(2,1)} %reshape.80) | copy-start | bytes 786436
  184.3 2.4 copy-start.14
  184.3 2.5 copy-start.17
  184.3 11.0 %copy-start.10 = (bf16[64,2048]{1,0:T(8,128)(2,1)S(1)}, bf16[64,2048]{1,0:T(8,128)(2,1)}, u32[]{:S(2)}) copy-start(bf16[64,2048]{1,0:T(8,128)(2,1)} %param.21) | copy-start | bytes 786436
  195.3 5.1 %copy-start.15 = (f32[2048]{0:T(1024)S(1)}, f32[2048]{0:T(1024)}, u32[]{:S(2)}) copy-start(f32[2048]{0:T(1024)} %param.32) | copy-start | bytes 24580
  201.3 194.0 %all-gather.15.cloned.1.call-start = ((), (), s32[]{:S(2)}) async-start(), calls=%async_computation.5 | async-start | bytes 6488064 | tf_op jit(solution)/shard_map/all_gather | solution.py:194
  201.9 225.4 %reduce-scatter.2.cloned.1.call-start = ((), (), s32[]{:S(2)}) async-start(), calls=%async_computation.6 | async-start | bytes 1310720 | tf_op jit(solution)/shard_map/reduce_scatter | solution.py:199
  301.0 94.4 %copy-start.19 = (bf16[256,2048]{1,0:T(8,128)(2,1)S(1)}, bf16[256,2048]{1,0:T(8,128)(2,1)}, u32[]{:S(2)}) copy-start(bf16[256,2048]{1,0:T(8,128)(2,1)} %all-gather.11.cloned.1.call-done) | copy-start | bytes 3145732
  (2 other events, 2.6 us)
Sparse Core Ops, SparseCore 0:
  8.9 60.9 all-gather.8
  72.1 119.2 all-gather.16
  193.6 90.9 all-gather.12
  286.0 14.8 all-gather.10
  303.0 92.2 all-gather.14
  404.3 22.9 reduce-scatter.1
